TPU v7x, 32 devices: a whole 2x2x4 slice. The times are simulated.
32 devices in a mesh: ep: 8 (over z, core), tp: 4 (over y, x).
Axes of the slice: x: 2, y: 2, z: 4, core: 2. Of those that a mesh axis runs over, the one named last changes fastest.
Arguments:
- tokens: bfloat16 [1024, 2048], P('ep'), may hold values from -6 to 6
- selected: int32 [8, 256], P(None, 'ep'), may hold values from -1 to 127, as said below
- affinity: float32 [8, 256], P(None, 'ep'), may hold values from 0.05 to 1
- w_gate: bfloat16 [8, 2048, 2048], P('ep', None, 'tp'), may hold values from -0.125 to 0.125
- w_up: bfloat16 [8, 2048, 2048], P('ep', None, 'tp'), may hold values from -0.125 to 0.125
- w_down: bfloat16 [8, 2048, 2048], P('ep', 'tp'), may hold values from -0.125 to 0.125
Outputs:
- combined: bfloat16 [1024, 2048], P('ep', 'tp')
Inputs may be any that keep to these rules, and one draw needn't show every extreme that they name: `selected`: row e holds 8 aligned groups of 32 entries; the live entries of group j are distinct positions within the j-th block of 128 tokens, stand at the front of the group and are followed by -1; each row has 128 live entries in all, the number in a group varies, and some group of every row is full.
All inputs are finite; a program needn't handle non-finite values.
Results may differ from a plain program's by a relative error of at most 0.015.
Values may be sent and summed in bfloat16 or wider, within the bound.
A program may use at most 64 MiB of HBM per device.

v0:
```python
import jax
import jax.numpy as jnp
from jax import lax
from jax.sharding import PartitionSpec as P


def per_device(tokens, selected, affinity, w_gate, w_up, w_down):
    ep_count = lax.axis_size("ep")
    local_tokens = tokens.shape[0]
    experts_here = w_gate.shape[0]
    slot_count = selected.shape[1]
    clamped = jnp.maximum(selected, 0)
    gathered = jnp.take(tokens, clamped, axis=0)
    arrived = lax.all_to_all(gathered, "ep", split_axis=0, concat_axis=1, tiled=True)
    gate_act = jnp.einsum("ecd,edf->ecf", arrived, w_gate, preferred_element_type=jnp.float32)
    up_act = jnp.einsum("ecd,edf->ecf", arrived, w_up, preferred_element_type=jnp.float32)
    hidden = (jax.nn.silu(gate_act) * up_act).astype(jnp.bfloat16)
    summed = lax.psum_scatter(
        jnp.einsum("efd,ecf->dec", w_down, hidden, preferred_element_type=jnp.float32).astype(
            jnp.bfloat16
        ),
        "tp",
        scatter_dimension=0,
        tiled=True,
    )
    summed = summed.reshape(summed.shape[0], experts_here, ep_count, slot_count)
    returned = lax.all_to_all(summed, "ep", split_axis=2, concat_axis=1, tiled=True)
    feature_cols = returned.shape[0]
    returned = returned.reshape(feature_cols, experts_here * ep_count * slot_count)
    weights = jnp.where(selected >= 0, affinity, jnp.zeros_like(affinity)).reshape(-1)
    scaled_rows = returned.astype(jnp.float32).T * weights[:, None]
    combined = (
        jnp.zeros((local_tokens, feature_cols), jnp.float32)
        .at[clamped.reshape(-1)]
        .add(scaled_rows)
    )
    return combined.astype(jnp.bfloat16)


def solution(mesh):
    placed = (
        P("ep", None),
        P(None, "ep"),
        P(None, "ep"),
        P("ep", None, "tp"),
        P("ep", None, "tp"),
        P("ep", "tp", None),
    )
    return jax.shard_map(
        per_device, mesh=mesh, in_specs=placed, out_specs=P("ep", "tp"), check_vma=False
    )
```

profile of v0, /device:TPU:0, one launch (start us, length us, event | category | flops | bytes accessed | tf_op | source)
XLA Modules:
  0.0 101.5 jit_solution(7033173364249277879)
XLA Ops:
  6.5 0.0 copy-start
  6.5 0.0 reduce-scatter.2.cloned.1.call-start
  6.5 0.8 broadcast_maximum_fusion
  7.4 0.7 broadcast_compare_fusion
  8.1 0.1 reshape.87
  8.2 3.5 %gather_fusion = bf16[256,2048]{1,0:T(8,128)(2,1)S(1)} fusion(bf16[128,2048]{1,0:T(8,128)(2,1)} %param.6, s32[1024]{0:T(1024)S(1)} %pad_clamp_fusion), kind=kCustom, calls=%fused_computation | custom fusion | bytes 2098176 | tf_op jit(solution)/shard_map/jit(_take)/gather | solution.py:13
  11.6 0.0 copy-start.3
  11.6 0.2 broadcast_select_fusion
  11.8 32.8 %all_to_all.8 = bf16[8,32,2048]{2,1,0:T(8,128)(2,1)S(1)} all-to-all(bf16[8,32,2048]{2,1,0:T(8,128)(2,1)S(1)} %broadcast_select_fusion), channel_id=1, replica_groups=mesh['ep'=8,'tp'=4] {'ep'}, dimensions={0} | all-to-all | bytes 2097152 | tf_op jit(solution)/shard_map/all_to_all | solution.py:14
  44.7 0.0 copy-done.3
  44.7 1.6 %fusion.4 = f32[256,512]{1,0:T(8,128)} fusion(bf16[256,2048]{1,0:T(8,128)(2,1)S(1)} %bitcast.34, bf16[1,2048,512]{2,1,0:T(8,128)(2,1)S(1)} %copy-done.3), kind=kOutput, calls=%fused_computation.7 | convolution fusion | flops 536870912 | bytes 3670016 | tf_op jit(solution)/shard_map/ecd,edf->ecf/dot_general | solution.py:15
  46.2 0.0 copy-done
  46.2 0.0 copy-start.1
  46.2 0.0 copy-start.2
  46.2 4.0 %fusion = bf16[2048,1,256]{0,2,1:T(8,128)(2,1)} fusion(bf16[1,512,2048]{2,1,0:T(8,128)(2,1)S(1)} %copy-done, bf16[256,2048]{1,0:T(8,128)(2,1)S(1)} %bitcast.35, bf16[1,2048,512]{2,1,0:T(8,128)(2,1)} %param.10, f32[256,512]{1,0:T(8,128)} %fusion.4), kind=kOutput, calls=%fused_computation.3 | convolution fusion | flops 1075052544 | bytes 6815744 | tf_op jit(solution)/shard_map/efd,ecf->dec/dot_general | solution.py:19
  50.3 0.0 reduce-scatter.2.cloned.1.call-update
  50.3 27.0 %reduce-scatter.2.cloned.1.call-done = bf16[512,1,256]{0,2,1:T(8,128)(2,1)} async-done(((bf16[2048,1,256]{0,2,1:T(8,128)(2,1)}), bf16[512,1,256]{0,2,1:T(8,128)(2,1)}) %reduce-scatter.2.cloned.1.call-update) | async-done | bytes 262160 | tf_op jit(solution)/shard_map/reduce_scatter | solution.py:18
  77.3 4.6 %all-to-all-start.1 = ((bf16[512,1,8,32]{0,3,1,2:T(8,128)(2,1)}), bf16[512,1,8,32]{0,3,1,2:T(8,128)(2,1)S(1)}, u32[]{:S(2)}, u32[]{:S(2)}) async-start(bf16[512,1,8,32]{0,3,1,2:T(8,128)(2,1)} %bitcast.36), calls=%async_computation.2 | async-start | bytes 524288 | tf_op jit(solution)/shard_map/all_to_all | solution.py:27
  81.9 0.1 reshape.78
  82.0 0.0 copy-done.1
  82.0 0.0 copy-done.2
  82.0 0.1 mul.24
  82.1 9.5 %all-to-all-done.1 = bf16[512,1,8,32]{0,3,1,2:T(8,128)(2,1)S(1)} async-done(((bf16[512,1,8,32]{0,3,1,2:T(8,128)(2,1)}), bf16[512,1,8,32]{0,3,1,2:T(8,128)(2,1)S(1)}, u32[]{:S(2)}, u32[]{:S(2)}) %all-to-all-start.1) | async-done | bytes 262176 | tf_op jit(solution)/shard_map/all_to_all | solution.py:27
  91.6 2.4 %scatter_custom_fusion = f32[128,512]{1,0:T(8,128)S(1)} fusion(s32[256]{0:T(256)S(1)} %bitcast.37, bf16[512,256]{0,1:T(8,128)(2,1)S(1)} %bitcast.33, f32[256]{0:T(256)S(1)} %mul.24, f32[]{:T(128)} %constant.9.clone.1), kind=kCustom, calls=%fused_computation.14 | custom fusion | flops 393216 | bytes 525316 | tf_op jit(solution)/shard_map/scatter-add | solution.py:35
  94.0 0.7 convert_element_type.28
  (3 shorter events, 0.0 us)
Async XLA Ops:
  6.5 39.7 %copy-start = (bf16[1,512,2048]{2,1,0:T(8,128)(2,1)S(1)}, bf16[1,512,2048]{2,1,0:T(8,128)(2,1)}, u32[]{:S(2)}) copy-start(bf16[1,512,2048]{2,1,0:T(8,128)(2,1)} %param.11) | copy-start | bytes 6291460
  6.5 70.8 %reduce-scatter.2.cloned.1.call-start = ((), (), s32[]{:S(2)}) async-start(), calls=%async_computation.3 | async-start | bytes 1310720 | tf_op jit(solution)/shard_map/reduce_scatter | solution.py:18
  11.6 33.0 %copy-start.3 = (bf16[1,2048,512]{2,1,0:T(8,128)(2,1)S(1)}, bf16[1,2048,512]{2,1,0:T(8,128)(2,1)}, u32[]{:S(2)}) copy-start(bf16[1,2048,512]{2,1,0:T(8,128)(2,1)} %param.9) | copy-start | bytes 6291460
  46.2 35.8 %copy-start.1 = (s32[8,32]{1,0:T(8,128)S(1)}, s32[8,32]{1,0:T(8,128)}, u32[]{:S(2)}) copy-start(s32[8,32]{1,0:T(8,128)} %param.7) | copy-start | bytes 3076
  46.2 35.8 %copy-start.2 = (f32[8,32]{1,0:T(8,128)S(1)}, f32[8,32]{1,0:T(8,128)}, u32[]{:S(2)}) copy-start(f32[8,32]{1,0:T(8,128)} %param.8) | copy-start | bytes 3076
  77.3 14.3 %all-to-all-start.1 = ((bf16[512,1,8,32]{0,3,1,2:T(8,128)(2,1)}), bf16[512,1,8,32]{0,3,1,2:T(8,128)(2,1)S(1)}, u32[]{:S(2)}, u32[]{:S(2)}) async-start(bf16[512,1,8,32]{0,3,1,2:T(8,128)(2,1)} %bitcast.36), calls=%async_computation.2 | async-start | bytes 524288 | tf_op jit(solution)/shard_map/all_to_all | solution.py:27
Sparse Core Ops, SparseCore 0:
  50.4 26.8 reduce-scatter.1
where the time goes:
time: 102 us
  waiting for transfers between devices  36.6 us (36%)
  blocking collectives  32.8 us (32%)
  between operations  13.4 us (13%)
  matrix products  5.59 us (5%)
  other arithmetic  4.75 us (5%)
  starting transfers between devices  4.62 us (5%)
  local copies, waits for them, and re-layouts  3.73 us (4%)
    all_to_all x1, blocking collectives, per_device(): lax.all_to_all(gathered, 'ep', split_axis=0, concat_axis=1, tiled=True)  32.8 us
    reduce_scatter x1, waiting for transfers between devices, per_device(): lax.psum_scatter(jnp.einsum('efd,ecf->dec', w_down, hidden, preferred_ele...  27 us
    all_to_all x1, waiting for transfers between devices, per_device(): lax.all_to_all(summed, 'ep', split_axis=2, concat_axis=1, tiled=True)  9.54 us
    all_to_all x1, starting transfers between devices, per_device(): lax.all_to_all(summed, 'ep', split_axis=2, concat_axis=1, tiled=True)  4.61 us
    dot_general x1, matrix products, per_device(): jnp.einsum('efd,ecf->dec', w_down, hidden, preferred_element_type=jnp.flo...  4.04 us
    gather x1, local copies, waits for them, and re-layouts, per_device(): gathered = jnp.take(tokens, clamped, axis=0)  3.48 us
    scatter-add x1, other arithmetic, per_device(): combined = jnp.zeros((local_tokens, feature_cols), jnp.float32).at[clampe...  2.37 us
  transfers between devices with their start and end apart: 2, of which 2 were waited for; matrix products, arithmetic and copies ran while one was open for 0% of the time, Pallas kernels for 0%

commit v1 on v0

--- a/solution.py
+++ b/solution.py
@@ -2,6 +2,13 @@
 import jax.numpy as jnp
 from jax import lax
 from jax.sharding import PartitionSpec as P
+
+
+def trade_parts(shard, axis, split, join):
+    peers = lax.axis_size(axis)
+    blocks = jnp.stack(jnp.split(shard, peers, axis=split), axis=0)
+    blocks = lax.all_to_all(blocks, axis, split_axis=0, concat_axis=0)
+    return jnp.concatenate(blocks, axis=join)
 
 
 def per_device(tokens, selected, affinity, w_gate, w_up, w_down):
@@ -24,7 +31,7 @@
         tiled=True,
     )
     summed = summed.reshape(summed.shape[0], experts_here, ep_count, slot_count)
-    returned = lax.all_to_all(summed, "ep", split_axis=2, concat_axis=1, tiled=True)
+    returned = trade_parts(summed, "ep", 2, 1)
     feature_cols = returned.shape[0]
     returned = returned.reshape(feature_cols, experts_here * ep_count * slot_count)
     weights = jnp.where(selected >= 0, affinity, jnp.zeros_like(affinity)).reshape(-1)

time: 102 us -> 113 us (1.11)
  local copies, waits for them, and re-layouts: 3.73 us -> 14.6 us
    unnamed x8 -> x15, local copies, waits for them, and re-layouts: 0.02 us -> 9.55 us
    another operation x0 -> x1, local copies, waits for them, and re-layouts: none -> 1.36 us  [trade_parts(): blocks = jnp.stack(jnp.split(shard, peers, axis=split), axis=0)]
where the time goes in v1:
time: 113 us; the launch traced here: 112 us
  waiting for transfers between devices  36.6 us (32%)
  blocking collectives  32.8 us (29%)
  local copies, waits for them, and re-layouts  14.6 us (13%)
  between operations  13.4 us (12%)
  matrix products  5.57 us (5%)
  other arithmetic  4.79 us (4%)
  starting transfers between devices  4.6 us (4%)
    all_to_all x1, blocking collectives, per_device(): lax.all_to_all(gathered, 'ep', split_axis=0, concat_axis=1, tiled=True)  32.8 us
    reduce_scatter x1, waiting for transfers between devices, per_device(): lax.psum_scatter(jnp.einsum('efd,ecf->dec', w_down, hidden, preferred_ele...  27 us
    unnamed x15, local copies, waits for them, and re-layouts  9.55 us
    all_to_all x1, waiting for transfers between devices, trade_parts(): blocks = lax.all_to_all(blocks, axis, split_axis=0, concat_axis=0)  9.54 us
    all_to_all x1, starting transfers between devices, trade_parts(): blocks = lax.all_to_all(blocks, axis, split_axis=0, concat_axis=0)  4.6 us
    dot_general x1, matrix products, per_device(): jnp.einsum('efd,ecf->dec', w_down, hidden, preferred_element_type=jnp.flo...  4.03 us
    gather x1, local copies, waits for them, and re-layouts, per_device(): gathered = jnp.take(tokens, clamped, axis=0)  3.48 us
    scatter-add x1, other arithmetic, per_device(): combined = jnp.zeros((local_tokens, feature_cols), jnp.float32).at[clampe...  2.31 us
  transfers between devices with their start and end apart: 2, of which 2 were waited for; matrix products, arithmetic and copies ran while one was open for 0% of the time, Pallas kernels for 0%

profile of v1, /device:TPU:0, one launch (start us, length us, event | category | flops | bytes accessed | tf_op | source)
XLA Modules:
  0.0 112.4 jit_solution(15528485477544004841)
XLA Ops:
  6.5 0.0 copy-start
  6.5 0.0 reduce-scatter.2.cloned.1.call-start
  6.5 0.8 broadcast_compare_fusion
  7.4 0.7 broadcast_maximum_fusion
  8.1 0.1 reshape.83
  8.2 3.5 %gather_fusion = bf16[256,2048]{1,0:T(8,128)(2,1)S(1)} fusion(bf16[128,2048]{1,0:T(8,128)(2,1)} %param.6, s32[1024]{0:T(1024)S(1)} %pad_clamp_fusion), kind=kCustom, calls=%fused_computation | custom fusion | bytes 2098176 | tf_op jit(solution)/shard_map/jit(_take)/gather | solution.py:20
  11.6 0.0 copy-start.3
  11.7 0.2 broadcast_select_fusion
  11.8 32.8 %all_to_all.14 = bf16[8,32,2048]{2,1,0:T(8,128)(2,1)S(1)} all-to-all(bf16[8,32,2048]{2,1,0:T(8,128)(2,1)S(1)} %broadcast_select_fusion), channel_id=1, replica_groups=mesh['ep'=8,'tp'=4] {'ep'}, dimensions={0} | all-to-all | bytes 2097152 | tf_op jit(solution)/shard_map/all_to_all | solution.py:21
  44.7 0.0 copy-done.3
  44.7 1.5 %fusion.4 = f32[256,512]{1,0:T(8,128)} fusion(bf16[256,2048]{1,0:T(8,128)(2,1)S(1)} %bitcast.65, bf16[1,2048,512]{2,1,0:T(8,128)(2,1)S(1)} %copy-done.3), kind=kOutput, calls=%fused_computation.7 | convolution fusion | flops 536870912 | bytes 3670016 | tf_op jit(solution)/shard_map/ecd,edf->ecf/dot_general | solution.py:22
  46.2 0.0 copy-done
  46.2 4.0 %fusion = bf16[2048,1,256]{0,2,1:T(8,128)(2,1)} fusion(bf16[1,512,2048]{2,1,0:T(8,128)(2,1)S(1)} %copy-done, bf16[256,2048]{1,0:T(8,128)(2,1)S(1)} %bitcast.66, bf16[1,2048,512]{2,1,0:T(8,128)(2,1)} %param.10, f32[256,512]{1,0:T(8,128)} %fusion.4), kind=kOutput, calls=%fused_computation.3 | convolution fusion | flops 1075052544 | bytes 6815744 | tf_op jit(solution)/shard_map/efd,ecf->dec/dot_general | solution.py:26
  50.3 0.0 reduce-scatter.2.cloned.1.call-update
  50.3 27.0 %reduce-scatter.2.cloned.1.call-done = bf16[512,1,256]{0,2,1:T(8,128)(2,1)} async-done(((bf16[2048,1,256]{0,2,1:T(8,128)(2,1)}), bf16[512,1,256]{0,2,1:T(8,128)(2,1)}) %reduce-scatter.2.cloned.1.call-update) | async-done | bytes 262160 | tf_op jit(solution)/shard_map/reduce_scatter | solution.py:25
  77.3 1.4 %fusion.30 = bf16[8,512,1,1,32]{1,4,3,2,0:T(8,128)(2,1)} fusion(bf16[512,1,8,32]{0,3,2,1:T(8,128)(2,1)} %bitcast.67), kind=kLoop, calls=%fused_computation.37 | loop fusion | bytes 65536
  78.7 1.4 %fusion.29 = bf16[8,512,1,1,32]{1,4,3,2,0:T(8,128)(2,1)} fusion(bf16[8,512,1,1,32]{1,4,3,2,0:T(8,128)(2,1)} %fusion.30, bf16[512,1,8,32]{0,3,2,1:T(8,128)(2,1)} %bitcast.68), kind=kLoop, calls=%fused_computation.35 | loop fusion | bytes 65536
  80.0 1.4 %fusion.28 = bf16[8,512,1,1,32]{1,4,3,2,0:T(8,128)(2,1)} fusion(bf16[8,512,1,1,32]{1,4,3,2,0:T(8,128)(2,1)} %fusion.29, bf16[512,1,8,32]{0,3,2,1:T(8,128)(2,1)} %bitcast.69), kind=kLoop, calls=%fused_computation.33 | loop fusion | bytes 65536
  81.4 1.4 %fusion.27 = bf16[8,512,1,1,32]{1,4,3,2,0:T(8,128)(2,1)} fusion(bf16[8,512,1,1,32]{1,4,3,2,0:T(8,128)(2,1)} %fusion.28, bf16[512,1,8,32]{0,3,2,1:T(8,128)(2,1)} %bitcast.70), kind=kLoop, calls=%fused_computation.31 | loop fusion | bytes 65536
  82.7 1.4 %fusion.26 = bf16[8,512,1,1,32]{1,4,3,2,0:T(8,128)(2,1)} fusion(bf16[8,512,1,1,32]{1,4,3,2,0:T(8,128)(2,1)} %fusion.27, bf16[512,1,8,32]{0,3,2,1:T(8,128)(2,1)} %bitcast.71), kind=kLoop, calls=%fused_computation.29 | loop fusion | bytes 65536
  84.1 1.4 %fusion.25 = bf16[8,512,1,1,32]{1,4,3,2,0:T(8,128)(2,1)} fusion(bf16[8,512,1,1,32]{1,4,3,2,0:T(8,128)(2,1)} %fusion.26, bf16[512,1,8,32]{0,3,2,1:T(8,128)(2,1)} %bitcast.72), kind=kLoop, calls=%fused_computation.27 | loop fusion | bytes 65536
  85.5 1.4 %fusion.24 = bf16[8,512,1,1,32]{1,4,3,2,0:T(8,128)(2,1)} fusion(bf16[8,512,1,1,32]{1,4,3,2,0:T(8,128)(2,1)} %fusion.25, bf16[512,1,8,32]{0,3,2,1:T(8,128)(2,1)} %bitcast.73), kind=kLoop, calls=%fused_computation.25 | loop fusion | bytes 65536
  86.8 1.4 %fusion.23 = bf16[8,512,1,1,32]{1,4,3,2,0:T(8,128)(2,1)} fusion(bf16[8,512,1,1,32]{1,4,3,2,0:T(8,128)(2,1)} %fusion.24, bf16[512,1,8,32]{0,3,2,1:T(8,128)(2,1)} %bitcast.74), kind=kLoop, calls=%fused_computation.23 | loop fusion | bytes 65536 | tf_op jit(solution)/shard_map/stack | solution.py:9
  88.2 4.6 %all-to-all-start.1 = ((bf16[8,512,1,1,32]{1,4,3,2,0:T(8,128)(2,1)}), bf16[8,512,1,1,32]{1,4,3,2,0:T(8,128)(2,1)S(1)}, u32[]{:S(2)}, u32[]{:S(2)}) async-start(bf16[8,512,1,1,32]{1,4,3,2,0:T(8,128)(2,1)} %fusion.23), calls=%async_computation.2 | async-start | bytes 524288 | tf_op jit(solution)/shard_map/all_to_all | solution.py:10
  92.8 0.1 reshape.74
  92.9 0.0 copy-done.1
  92.9 0.0 copy-done.2
  92.9 0.1 mul.24
  93.0 9.5 %all-to-all-done.1 = bf16[8,512,1,1,32]{1,4,3,2,0:T(8,128)(2,1)S(1)} async-done(((bf16[8,512,1,1,32]{1,4,3,2,0:T(8,128)(2,1)}), bf16[8,512,1,1,32]{1,4,3,2,0:T(8,128)(2,1)S(1)}, u32[]{:S(2)}, u32[]{:S(2)}) %all-to-all-start.1) | async-done | bytes 262176 | tf_op jit(solution)/shard_map/all_to_all | solution.py:10
  102.5 0.1 bitcast_multiply_fusion
  102.6 2.3 %scatter_custom_fusion = f32[128,512]{1,0:T(8,128)S(1)} fusion(s32[256]{0:T(256)S(1)} %bitcast.75, f32[512,256]{0,1:T(8,128)S(1)} %bitcast_multiply_fusion, f32[]{:T(128)} %constant.9.clone.1), kind=kCustom, calls=%fused_computation.13 | custom fusion | flops 131072 | bytes 786436 | tf_op jit(solution)/shard_map/scatter-add | solution.py:42
  104.9 0.7 convert_element_type.32
  (5 shorter events, 0.0 us)
Async XLA Ops:
  6.5 39.7 %copy-start = (bf16[1,512,2048]{2,1,0:T(8,128)(2,1)S(1)}, bf16[1,512,2048]{2,1,0:T(8,128)(2,1)}, u32[]{:S(2)}) copy-start(bf16[1,512,2048]{2,1,0:T(8,128)(2,1)} %param.11) | copy-start | bytes 6291460
  6.5 70.8 %reduce-scatter.2.cloned.1.call-start = ((), (), s32[]{:S(2)}) async-start(), calls=%async_computation.3 | async-start | bytes 1310720 | tf_op jit(solution)/shard_map/reduce_scatter | solution.py:25
  11.6 33.0 %copy-start.3 = (bf16[1,2048,512]{2,1,0:T(8,128)(2,1)S(1)}, bf16[1,2048,512]{2,1,0:T(8,128)(2,1)}, u32[]{:S(2)}) copy-start(bf16[1,2048,512]{2,1,0:T(8,128)(2,1)} %param.9) | copy-start | bytes 6291460
  50.2 42.6 %copy-start.1 = (s32[8,32]{1,0:T(8,128)S(1)}, s32[8,32]{1,0:T(8,128)}, u32[]{:S(2)}) copy-start(s32[8,32]{1,0:T(8,128)} %param.7) | copy-start | bytes 3076
  50.3 42.6 %copy-start.2 = (f32[8,32]{1,0:T(8,128)S(1)}, f32[8,32]{1,0:T(8,128)}, u32[]{:S(2)}) copy-start(f32[8,32]{1,0:T(8,128)} %param.8) | copy-start | bytes 3076
  88.2 14.3 %all-to-all-start.1 = ((bf16[8,512,1,1,32]{1,4,3,2,0:T(8,128)(2,1)}), bf16[8,512,1,1,32]{1,4,3,2,0:T(8,128)(2,1)S(1)}, u32[]{:S(2)}, u32[]{:S(2)}) async-start(bf16[8,512,1,1,32]{1,4,3,2,0:T(8,128)(2,1)} %fusion.23), calls=%async_computation.2 | async-start | bytes 524288 | tf_op jit(solution)/shard_map/all_to_all | solution.py:10
Sparse Core Ops, SparseCore 0:
  50.4 26.8 reduce-scatter.1
